TPU v7x, 32 devices: a whole 2x2x4 slice. The times are simulated.
32 devices in a mesh: ep: 8 (over z, x), tp: 4 (over y, core).
Axes of the slice: x: 2, y: 2, z: 4, core: 2. Of those that a mesh axis runs over, the one named last changes fastest.
Arguments:
- conv_gate: bfloat16 [4096, 2048], P('ep', 'tp'), may hold values from -6 to 6
- conv_in_gate: bfloat16 [4096, 2048], P('ep', 'tp'), may hold values from -6 to 6
- conv_value: bfloat16 [4096, 2048], P('ep', 'tp'), may hold values from -6 to 6
- conv_taps: float32 [3, 2048], P(None, 'tp'), may hold values from -3.5 to 3.5
- mix_out_weight: bfloat16 [2048, 4096], P(None, 'tp'), may hold values from -0.125 to 0.125
- expert_input: bfloat16 [1280, 4096], P('ep', 'tp'), may hold values from -1600 to 1600
- expert_gain: float32 [4096], replicated, may hold values from 0.1 to 1.9
- routes: int32 [1280, 2], P('ep'), may hold values from 0 to 7, all different within a row; in each aligned block of 160 rows (0 to 159, 160 to 319, ...) at most 60 rows name the same one
- group_prob: float32 [1280], P('ep'), may hold values from 0.3 to 1
- pair_logits: float32 [1280, 2], P('ep'), may hold values from -6 to 6
- expert_gate: bfloat16 [8, 4096, 2048], P('ep', None, 'tp'), may hold values from -0.09375 to 0.09375
- expert_up: bfloat16 [8, 4096, 2048], P('ep', None, 'tp'), may hold values from -0.09375 to 0.09375
- expert_down: bfloat16 [8, 2048, 4096], P('ep', None, 'tp'), may hold values from -0.125 to 0.125
Outputs:
- mixed: bfloat16 [4096, 4096], P('ep', 'tp')
- expert_output: bfloat16 [1280, 4096], P('ep', 'tp')
Inputs may be any that keep to these rules, and one draw needn't show every extreme that they name: `routes`: in the 160 rows of one index of ep no expert is named by more than 60 rows, a bound that some block reaches; each row names 2 different experts.
All inputs are finite; a program needn't handle non-finite values.
Results may differ from a plain program's by a relative error of at most 0.0071.
Values may be sent and summed in bfloat16 or wider, within the bound.
No kernel may reach another device: no remote copies, remote signals or barrier semaphores. Data moves between devices by JAX's collectives and lax.ppermute only.
A program may use at most 64 MiB of HBM per device.

v0:
```python
import jax
import jax.numpy as jnp
from jax import lax
from jax.sharding import PartitionSpec as P

D = 4096
EPS = 1e-06


def shifted(block, axis, distance):
    devices = range(lax.axis_size(axis))
    route = [(i - distance, i) for i in devices if i - distance in devices]
    return lax.ppermute(block, axis, route)


def slot_table(route_block, capacity, expert_count):
    pair_ids = route_block.reshape(-1)
    onehot = (pair_ids[:, None] == jnp.arange(expert_count, dtype=jnp.int32)[None, :]).astype(
        jnp.int32
    )
    earlier = jnp.cumsum(onehot, axis=0) - onehot
    within = jnp.sum(earlier * onehot, axis=1)
    return pair_ids * capacity + within


def pair_weights(group_prob, pair_logits):
    spread = pair_logits[:, 0] - pair_logits[:, 1]
    return (
        jnp.stack([jax.nn.sigmoid(spread), jax.nn.sigmoid(-spread)], axis=1) * group_prob[:, None]
    )


def per_device(
    conv_gate,
    conv_in_gate,
    conv_value,
    conv_taps,
    mix_out_weight,
    expert_input,
    expert_gain,
    routes,
    group_prob,
    pair_logits,
    expert_gate,
    expert_up,
    expert_down,
):
    reach = conv_taps.shape[0] - 1
    token_rows = conv_value.shape[0]
    products = conv_in_gate.astype(jnp.float32) * conv_value.astype(jnp.float32)
    earlier_rows = shifted(products[token_rows - reach :], "ep", 1)
    padded = jnp.concatenate([earlier_rows, products], axis=0)
    convolved = jnp.zeros_like(products)
    for offset in range(reach + 1):
        convolved = convolved + conv_taps[offset][None, :] * padded[offset : offset + token_rows]
    mixer_rows = (conv_gate.astype(jnp.float32) * convolved).astype(jnp.bfloat16)
    mixed = jnp.dot(
        lax.all_gather(mixer_rows, "tp", axis=1, tiled=True),
        mix_out_weight,
        preferred_element_type=jnp.float32,
    ).astype(jnp.bfloat16)
    expert_count = lax.axis_size("ep")
    tok_rows, choose_count = routes.shape
    capacity = 3 * tok_rows * choose_count // (2 * expert_count)
    slot_index = slot_table(routes, capacity, expert_count)
    pair_row = jnp.arange(tok_rows * choose_count, dtype=jnp.int32) // choose_count
    slot_rows = expert_count * capacity
    gate_block = expert_gate[0]
    up_block = expert_up[0]
    down_block = expert_down[0]
    columns = expert_input.shape[1]
    features = expert_input.astype(jnp.float32)
    squares = lax.psum(jnp.sum(features * features, axis=1), "tp")
    scale = lax.rsqrt(squares / D + EPS)
    gain_part = lax.dynamic_slice_in_dim(expert_gain, lax.axis_index("tp") * columns, columns, 0)
    normed = (features * scale[:, None] * gain_part[None, :]).astype(jnp.bfloat16)
    buffer = jnp.zeros((slot_rows, columns), jnp.bfloat16).at[slot_index].set(normed[pair_row])
    arrived = lax.all_to_all(
        buffer.reshape(expert_count, capacity, columns),
        "ep",
        split_axis=0,
        concat_axis=0,
        tiled=True,
    ).reshape(slot_rows, columns)
    shard_piece = lax.all_gather(arrived, "tp", axis=1, tiled=True)
    gate_sum = jnp.dot(shard_piece, gate_block, preferred_element_type=jnp.float32)
    up_sum = jnp.dot(shard_piece, up_block, preferred_element_type=jnp.float32)
    hidden = (jax.nn.silu(gate_sum) * up_sum).astype(jnp.bfloat16)
    results = jnp.dot(
        lax.all_gather(hidden, "tp", axis=1, tiled=True),
        down_block,
        preferred_element_type=jnp.float32,
    ).astype(jnp.bfloat16)
    returned = lax.all_to_all(
        results.reshape(expert_count, capacity, down_block.shape[1]),
        "ep",
        split_axis=0,
        concat_axis=0,
        tiled=True,
    ).reshape(slot_rows, down_block.shape[1])
    picked = (
        returned[slot_index]
        .reshape(tok_rows, choose_count, down_block.shape[1])
        .astype(jnp.float32)
    )
    weights = pair_weights(group_prob, pair_logits)
    expert_output = jnp.sum(picked * weights[:, :, None], axis=1).astype(jnp.bfloat16)
    return (mixed, expert_output)


def solution(mesh):
    in_specs = (
        P("ep", "tp"),
        P("ep", "tp"),
        P("ep", "tp"),
        P(None, "tp"),
        P(None, "tp"),
        P("ep", "tp"),
        P(),
        P("ep", None),
        P("ep"),
        P("ep", None),
        P("ep", None, "tp"),
        P("ep", None, "tp"),
        P("ep", None, "tp"),
    )
    out_specs = (P("ep", "tp"), P("ep", "tp"))
    return jax.shard_map(
        per_device, mesh=mesh, in_specs=in_specs, out_specs=out_specs, check_vma=False
    )
```

profile of v0, /device:TPU:0, one launch (start us, length us, event | category | flops | bytes accessed | tf_op | source)
XLA Modules:
  0.0 170.7 jit_solution(3366997663291530493)
XLA Ops:
  7.2 0.0 all-gather.6.cloned.1.call-start
  7.2 0.8 copy.17
  8.0 0.7 broadcast_multiply_fusion
  8.7 0.1 eq.22
  8.9 0.9 reduce-window.6
  9.8 0.2 slice_reduce_fusion
  10.0 0.1 add_bitcast_fusion
  10.1 0.1 copy.16
  10.2 0.1 mul.117
  10.4 1.1 fusion.22
  11.5 8.4 %psum.7 = f32[160]{0:T(256)S(1)} all-reduce(f32[160]{0:T(256)S(1)} %fusion.22), channel_id=1, replica_groups=mesh['ep'=8,'tp'=4] {'tp'}, use_global_device_ids=true, to_apply=%region_4.5 | all-reduce | flops 160 | bytes 1280 | tf_op jit(solution)/shard_map/psum | solution.py:73
  19.9 0.7 dynamic_slice.3
  20.6 1.1 fusion.24
  21.8 4.5 %scatter_custom_fusion = bf16[480,1024]{1,0:T(8,128)(2,1)S(1)} fusion(s32[320]{0:T(512)S(1)} %fusion.30, bf16[160,1024]{1,0:T(8,128)(2,1)S(1)} %fusion.24, s32[1024]{0:T(1024)S(1)} %pad_clamp_fusion.1, bf16[]{:T(256)} %constant.18.clone.1), kind=kCustom, calls=%fused_computation.30 | custom fusion | bytes 983042 | tf_op jit(solution)/shard_map/scatter | solution.py:77
  26.2 0.2 reshape.137
  26.4 30.1 %all_to_all.10 = bf16[8,60,1024]{2,1,0:T(8,128)(2,1)S(1)} all-to-all(bf16[8,60,1024]{2,1,0:T(8,128)(2,1)S(1)} %reshape.137), channel_id=1, replica_groups=mesh['ep'=8,'tp'=4] {'ep'}, dimensions={0} | all-to-all | bytes 1966080 | tf_op jit(solution)/shard_map/all_to_all | solution.py:78
  56.6 1.1 reshape.138
  57.7 0.0 all-gather.6.cloned.1.call-update
  57.7 0.0 all-gather.8.cloned.1.call-start
  57.8 32.1 %all-gather.6.cloned.1.call-done = bf16[480,4096]{1,0:T(8,128)(2,1)} async-done(((bf16[480,1024]{1,0:T(8,128)(2,1)}), bf16[480,4096]{1,0:T(8,128)(2,1)}) %all-gather.6.cloned.1.call-update) | async-done | bytes 3932176 | tf_op jit(solution)/shard_map/all_gather | solution.py:85
  89.9 5.7 %fusion.4 = f32[480,512]{1,0:T(8,128)S(1)} fusion(bf16[480,4096]{1,0:T(8,128)(2,1)} %all-gather.6.cloned.1.call-done, bf16[1,4096,512]{2,1,0:T(8,128)(2,1)} %param.23), kind=kOutput, calls=%fused_computation.7 | convolution fusion | flops 2013265920 | bytes 9109504 | tf_op jit(solution)/shard_map/dot_general | solution.py:86
  95.6 0.0 copy-done.6
  95.6 0.0 copy-done.7
  95.7 3.0 %fusion.12 = bf16[480,512]{1,0:T(8,128)(2,1)} fusion(bf16[480,4096]{1,0:T(8,128)(2,1)S(1)} %copy-done.7, bf16[1,4096,512]{2,1,0:T(8,128)(2,1)S(1)} %copy-done.6, f32[480,512]{1,0:T(8,128)S(1)} %fusion.4), kind=kOutput, calls=%fused_computation.13 | convolution fusion | flops 2014740480 | bytes 9601024 | tf_op jit(solution)/shard_map/dot_general | solution.py:87
  98.7 0.0 all-gather.8.cloned.1.call-update
  98.8 0.0 all-gather.4.cloned.1.call-start
  98.8 0.0 copy-done.1
  98.8 0.0 copy-done.2
  98.8 0.1 convert_multiply_fusion
  99.0 3.4 %collective-permute-start = (f32[2,512]{1,0:T(2,128)S(1)}, f32[2,512]{1,0:T(2,128)S(1)}, u32[]{:S(2)}, u32[]{:S(2)}) collective-permute-start(f32[2,512]{1,0:T(2,128)S(1)} %slice.48), channel_id=1, source_target_pairs={{0,4},{4,8},{8,12},{12,16},{16,20},{20,24},{24,28},{1,5},{5,9},{9,... | collective-permute-start | bytes 12296 | tf_op jit(solution)/shard_map/ppermute | solution.py:13
  102.4 1.3 collective-permute-done
  103.7 0.0 copy-done
  103.7 1.2 fusion.20
  104.9 0.0 all-gather.4.cloned.1.call-update
  104.9 15.8 %all-gather.8.cloned.1.call-done = bf16[480,2048]{1,0:T(8,128)(2,1)} async-done(((bf16[480,512]{1,0:T(8,128)(2,1)}), bf16[480,2048]{1,0:T(8,128)(2,1)}) %all-gather.8.cloned.1.call-update) | async-done | bytes 1966096 | tf_op jit(solution)/shard_map/all_gather | solution.py:90
  120.8 5.0 %fusion.6 = bf16[480,1024]{1,0:T(8,128)(2,1)S(1)} fusion(bf16[480,2048]{1,0:T(8,128)(2,1)} %all-gather.8.cloned.1.call-done, bf16[1,2048,1024]{2,1,0:T(8,128)(2,1)} %param.25), kind=kOutput, calls=%fused_computation.10 | convolution fusion | flops 2013757440 | bytes 7143424 | tf_op jit(solution)/shard_map/dot_general | solution.py:89
  125.7 0.0 copy-start.4
  125.8 0.0 copy-start.5
  125.8 1.2 reshape.139
  126.9 5.5 %all-to-all-start.1 = ((bf16[8,60,1024]{2,1,0:T(8,128)(2,1)}), bf16[8,60,1024]{2,1,0:T(8,128)(2,1)S(1)}, u32[]{:S(2)}, u32[]{:S(2)}) async-start(bf16[8,60,1024]{2,1,0:T(8,128)(2,1)} %reshape.139), calls=%async_computation.1 | async-start | bytes 2097152 | tf_op jit(solution)/shard_map/all_to_all | solution.py:94
  132.5 0.1 copy.18
  132.6 12.9 %all-gather.4.cloned.1.call-done = bf16[512,2048]{1,0:T(8,128)(2,1)} async-done(((bf16[512,512]{1,0:T(8,128)(2,1)}), bf16[512,2048]{1,0:T(8,128)(2,1)}) %all-gather.4.cloned.1.call-update) | async-done | bytes 2097168 | tf_op jit(solution)/shard_map/all_gather | solution.py:58
  145.5 6.1 %convolution_convert_fusion = bf16[512,1024]{1,0:T(8,128)(2,1)} fusion(bf16[512,2048]{1,0:T(8,128)(2,1)} %all-gather.4.cloned.1.call-done, bf16[2048,1024]{1,0:T(8,128)(2,1)} %param.17), kind=kOutput, calls=%fused_computation.9 | convolution fusion | flops 2148007936 | bytes 7340032 | tf_op jit(solution)/shard_map/dot_general | solution.py:57
  151.6 7.0 %all-to-all-done.1 = bf16[8,60,1024]{2,1,0:T(8,128)(2,1)S(1)} async-done(((bf16[8,60,1024]{2,1,0:T(8,128)(2,1)}), bf16[8,60,1024]{2,1,0:T(8,128)(2,1)S(1)}, u32[]{:S(2)}, u32[]{:S(2)}) %all-to-all-start.1) | async-done | bytes 983072 | tf_op jit(solution)/shard_map/all_to_all | solution.py:94
  158.6 0.2 reshape.140
  158.8 2.1 %gather_fusion = bf16[320,1024]{1,0:T(8,128)(2,1)S(1)} fusion(bf16[480,1024]{1,0:T(8,128)(2,1)S(1)} %reshape.140, s32[1024]{0:T(1024)S(1)} %pad_clamp_fusion), kind=kCustom, calls=%fused_computation.1 | custom fusion | bytes 1312000 | tf_op jit(solution)/shard_map/gather | solution.py:102
  160.9 0.8 reshape.142
  161.7 2.4 %multiply_reduce_fusion = bf16[160,1024]{1,0:T(8,128)(2,1)} fusion(f32[160,2,1024]{2,1,0:T(2,128)S(1)} %reshape.142, f32[160,2]{1,0:T(8,128)S(1)} %copy.18), kind=kLoop, calls=%fused_computation.12 | loop fusion | flops 491520 | bytes 1639680 | tf_op jit(solution)/shard_map/reduce_sum | solution.py:107
  (23 shorter events, 0.2 us)
Async XLA Ops:
  7.2 82.8 %all-gather.6.cloned.1.call-start = ((), (), s32[]{:S(2)}) async-start(), calls=%async_computation.3 | async-start | bytes 4915200 | tf_op jit(solution)/shard_map/all_gather | solution.py:85
  57.7 63.0 %all-gather.8.cloned.1.call-start = ((), (), s32[]{:S(2)}) async-start(), calls=%async_computation.4 | async-start | bytes 2457600 | tf_op jit(solution)/shard_map/all_gather | solution.py:90
  89.9 5.7 %copy-start.6 = (bf16[1,4096,512]{2,1,0:T(8,128)(2,1)S(1)}, bf16[1,4096,512]{2,1,0:T(8,128)(2,1)}, u32[]{:S(2)}) copy-start(bf16[1,4096,512]{2,1,0:T(8,128)(2,1)} %param.24) | copy-start | bytes 12582916
  89.9 5.8 %copy-start.7 = (bf16[480,4096]{1,0:T(8,128)(2,1)S(1)}, bf16[480,4096]{1,0:T(8,128)(2,1)}, u32[]{:S(2)}) copy-start(bf16[480,4096]{1,0:T(8,128)(2,1)} %all-gather.6.cloned.1.call-done) | copy-start | bytes 11796484
  95.7 3.1 %copy-start.1 = (bf16[512,512]{1,0:T(8,128)(2,1)S(1)}, bf16[512,512]{1,0:T(8,128)(2,1)}, u32[]{:S(2)}) copy-start(bf16[512,512]{1,0:T(8,128)(2,1)} %param.15) | copy-start | bytes 1572868
  95.7 3.1 %copy-start.2 = (bf16[512,512]{1,0:T(8,128)(2,1)S(1)}, bf16[512,512]{1,0:T(8,128)(2,1)}, u32[]{:S(2)}) copy-start(bf16[512,512]{1,0:T(8,128)(2,1)} %param.14) | copy-start | bytes 1572868
  95.7 6.7 %copy-start.3 = (f32[3,512]{1,0:T(4,128)S(1)}, f32[3,512]{1,0:T(4,128)}, u32[]{:S(2)}) copy-start(f32[3,512]{1,0:T(4,128)} %param.16) | copy-start | bytes 18436
  95.7 8.0 %copy-start = (bf16[512,512]{1,0:T(8,128)(2,1)S(1)}, bf16[512,512]{1,0:T(8,128)(2,1)}, u32[]{:S(2)}) copy-start(bf16[512,512]{1,0:T(8,128)(2,1)} %param.13) | copy-start | bytes 1572868
  98.8 46.7 %all-gather.4.cloned.1.call-start = ((), (), s32[]{:S(2)}) async-start(), calls=%async_computation.2 | async-start | bytes 2621440 | tf_op jit(solution)/shard_map/all_gather | solution.py:58
  99.0 4.7 %collective-permute-start = (f32[2,512]{1,0:T(2,128)S(1)}, f32[2,512]{1,0:T(2,128)S(1)}, u32[]{:S(2)}, u32[]{:S(2)}) collective-permute-start(f32[2,512]{1,0:T(2,128)S(1)} %slice.48), channel_id=1, source_target_pairs={{0,4},{4,8},{8,12},{12,16},{16,20},{20,24},{24,28},{1,5},{5,9},{9,... | collective-permute-start | bytes 12296 | tf_op jit(solution)/shard_map/ppermute | solution.py:13
  125.7 6.7 %copy-start.4 = (f32[160,2]{0,1:T(2,128)S(1)}, f32[160,2]{0,1:T(2,128)}, u32[]{:S(2)}) copy-start(f32[160,2]{0,1:T(2,128)} %param.22) | copy-start | bytes 3844
  125.8 6.7 %copy-start.5 = (f32[160]{0:T(256)S(1)}, f32[160]{0:T(256)}, u32[]{:S(2)}) copy-start(f32[160]{0:T(256)} %param.21) | copy-start | bytes 1924
  126.9 31.7 %all-to-all-start.1 = ((bf16[8,60,1024]{2,1,0:T(8,128)(2,1)}), bf16[8,60,1024]{2,1,0:T(8,128)(2,1)S(1)}, u32[]{:S(2)}, u32[]{:S(2)}) async-start(bf16[8,60,1024]{2,1,0:T(8,128)(2,1)} %reshape.139), calls=%async_computation.1 | async-start | bytes 2097152 | tf_op jit(solution)/shard_map/all_to_all | solution.py:94
Sparse Core Ops, SparseCore 0:
  57.8 32.0 all-gather.5
  98.9 21.8 all-gather.7
  122.9 22.5 all-gather.3
where the time goes:
time: 171 us
  waiting for transfers between devices  69.2 us (40%)
  blocking collectives  38.5 us (23%)
  matrix products  19.9 us (12%)
  between operations  14 us (8%)
  local copies, waits for them, and re-layouts  12.3 us (7%)
  starting transfers between devices  9 us (5%)
  other arithmetic  7.81 us (5%)
    all_gather x1, waiting for transfers between devices, per_device(): shard_piece = lax.all_gather(arrived, 'tp', axis=1, tiled=True)  32.1 us
    all_to_all x1, blocking collectives, per_device(): lax.all_to_all(buffer.reshape(expert_count, capacity, columns), 'ep', spl...  30.1 us
    all_gather x1, waiting for transfers between devices, per_device(): lax.all_gather(hidden, 'tp', axis=1, tiled=True)  15.8 us
    all_gather x1, waiting for transfers between devices, per_device(): lax.all_gather(mixer_rows, 'tp', axis=1, tiled=True)  12.9 us
    psum x1, blocking collectives, per_device(): squares = lax.psum(jnp.sum(features * features, axis=1), 'tp')  8.39 us
    all_to_all x1, waiting for transfers between devices, per_device(): lax.all_to_all(results.reshape(expert_count, capacity, down_block.shape[1...  6.98 us
    dot_general x1, matrix products, per_device(): jnp.dot(lax.all_gather(mixer_rows, 'tp', axis=1, tiled=True), mix_out_wei...  6.12 us
    dot_general x1, matrix products, per_device(): jnp.dot(shard_piece, gate_block, preferred_element_type=jnp.float32)  5.71 us
  transfers between devices with their start and end apart: 5, of which 5 were waited for; matrix products, arithmetic and copies ran while one was open for 8% of the time, Pallas kernels for 0%

commit v1 on v0

--- a/solution.py
+++ b/solution.py
@@ -82,7 +82,7 @@
         concat_axis=0,
         tiled=True,
     ).reshape(slot_rows, columns)
-    shard_piece = lax.all_gather(arrived, "tp", axis=1, tiled=True)
+    shard_piece = jnp.concatenate(lax.all_gather(arrived, "tp"), axis=1)
     gate_sum = jnp.dot(shard_piece, gate_block, preferred_element_type=jnp.float32)
     up_sum = jnp.dot(shard_piece, up_block, preferred_element_type=jnp.float32)
     hidden = (jax.nn.silu(gate_sum) * up_sum).astype(jnp.bfloat16)

time: 171 us -> 171 us (level)
  matrix products: 19.9 us -> 16.3 us
  local copies, waits for them, and re-layouts: 12.3 us -> 15.6 us
    dot_general x1, matrix products: 5.71 us -> 2.19 us  [per_device(): jnp.dot(shard_piece, gate_block, preferred_element_type=jnp.float32)]
where the time goes in v1:
time: 171 us; the launch traced here: 170 us
  waiting for transfers between devices  69.2 us (40%)
  blocking collectives  38.5 us (23%)
  matrix products  16.3 us (10%)
  local copies, waits for them, and re-layouts  15.6 us (9%)
  between operations  14 us (8%)
  starting transfers between devices  9 us (5%)
  other arithmetic  7.81 us (5%)
    all_gather x1, waiting for transfers between devices, per_device(): shard_piece = jnp.concatenate(lax.all_gather(arrived, 'tp'), axis=1)  32.1 us
    all_to_all x1, blocking collectives, per_device(): lax.all_to_all(buffer.reshape(expert_count, capacity, columns), 'ep', spl...  30.1 us
    all_gather x1, waiting for transfers between devices, per_device(): lax.all_gather(hidden, 'tp', axis=1, tiled=True)  15.8 us
    all_gather x1, waiting for transfers between devices, per_device(): lax.all_gather(mixer_rows, 'tp', axis=1, tiled=True)  12.9 us
    psum x1, blocking collectives, per_device(): squares = lax.psum(jnp.sum(features * features, axis=1), 'tp')  8.39 us
    all_to_all x1, waiting for transfers between devices, per_device(): lax.all_to_all(results.reshape(expert_count, capacity, down_block.shape[1...  6.98 us
    dot_general x1, matrix products, per_device(): jnp.dot(lax.all_gather(mixer_rows, 'tp', axis=1, tiled=True), mix_out_wei...  6.12 us
    all_to_all x1, starting transfers between devices, per_device(): lax.all_to_all(results.reshape(expert_count, capacity, down_block.shape[1...  5.51 us
  transfers between devices with their start and end apart: 5, of which 5 were waited for; matrix products, arithmetic and copies ran while one was open for 8% of the time, Pallas kernels for 0%

profile of v1, /device:TPU:0, one launch (start us, length us, event | category | flops | bytes accessed | tf_op | source)
XLA Modules:
  0.0 170.5 jit_solution(1417168286894958634)
XLA Ops:
  7.2 0.0 all-gather.6.cloned.1.call-start
  7.2 0.8 copy.21
  8.0 0.7 broadcast_multiply_fusion
  8.7 0.1 eq.22
  8.9 0.9 reduce-window.6
  9.8 0.2 slice_reduce_fusion
  10.0 0.1 add_bitcast_fusion
  10.1 0.1 copy.20
  10.2 0.1 mul.117
  10.4 1.1 fusion.22
  11.5 8.4 %psum.7 = f32[160]{0:T(256)S(1)} all-reduce(f32[160]{0:T(256)S(1)} %fusion.22), channel_id=1, replica_groups=mesh['ep'=8,'tp'=4] {'tp'}, use_global_device_ids=true, to_apply=%region_4.5 | all-reduce | flops 160 | bytes 1280 | tf_op jit(solution)/shard_map/psum | solution.py:73
  19.9 0.7 dynamic_slice.3
  20.6 1.1 fusion.24
  21.8 4.5 %scatter_custom_fusion = bf16[480,1024]{1,0:T(8,128)(2,1)S(1)} fusion(s32[320]{0:T(512)S(1)} %fusion.30, bf16[160,1024]{1,0:T(8,128)(2,1)S(1)} %fusion.24, s32[1024]{0:T(1024)S(1)} %pad_clamp_fusion.1, bf16[]{:T(256)} %constant.18.clone.1), kind=kCustom, calls=%fused_computation.30 | custom fusion | bytes 983042 | tf_op jit(solution)/shard_map/scatter | solution.py:77
  26.2 0.2 reshape.140
  26.4 30.1 %all_to_all.10 = bf16[8,60,1024]{2,1,0:T(8,128)(2,1)S(1)} all-to-all(bf16[8,60,1024]{2,1,0:T(8,128)(2,1)S(1)} %reshape.140), channel_id=1, replica_groups=mesh['ep'=8,'tp'=4] {'ep'}, dimensions={0} | all-to-all | bytes 1966080 | tf_op jit(solution)/shard_map/all_to_all | solution.py:78
  56.6 1.1 all_gather_reshape.3
  57.7 0.0 all-gather.6.cloned.1.call-update
  57.7 0.0 all-gather.8.cloned.1.call-start
  57.8 32.1 %all-gather.6.cloned.1.call-done = bf16[4,480,1024]{2,1,0:T(8,128)(2,1)} async-done(((bf16[1,480,1024]{2,1,0:T(8,128)(2,1)}), bf16[4,480,1024]{2,1,0:T(8,128)(2,1)}) %all-gather.6.cloned.1.call-update) | async-done | bytes 3932176 | tf_op jit(solution)/shard_map/all_gather | solution.py:85
  89.9 2.7 %copy.24 = bf16[4,60,8,1024]{3,2,0,1:T(8,128)(2,1)S(1)} copy(bf16[4,60,8,1024]{3,2,1,0:T(8,128)(2,1)} %bitcast.33) | data formatting | bytes 7864320 | tf_op jit(solution)/shard_map/reshape | solution.py:85
  92.6 0.7 copy-done.6
  93.3 2.2 %fusion.4 = f32[480,512]{1,0:T(8,128)S(1)} fusion(bf16[480,4096]{1,0:T(8,128)(2,1)S(1)} %bitcast.34, bf16[1,4096,512]{2,1,0:T(8,128)(2,1)S(1)} %copy-done.6), kind=kOutput, calls=%fused_computation.7 | convolution fusion | flops 2013265920 | bytes 9109504 | tf_op jit(solution)/shard_map/dot_general | solution.py:86
  95.5 0.0 copy-start.1
  95.5 0.0 copy-start.2
  95.5 0.0 copy-start.3
  95.5 0.0 copy-start
  95.5 3.0 %fusion.12 = bf16[480,512]{1,0:T(8,128)(2,1)} fusion(bf16[480,4096]{1,0:T(8,128)(2,1)S(1)} %bitcast.35, bf16[1,4096,512]{2,1,0:T(8,128)(2,1)S(1)} %copy-done.7, f32[480,512]{1,0:T(8,128)S(1)} %fusion.4), kind=kOutput, calls=%fused_computation.13 | convolution fusion | flops 2014740480 | bytes 9601024 | tf_op jit(solution)/shard_map/dot_general | solution.py:87
  98.6 0.0 all-gather.8.cloned.1.call-update
  98.6 0.0 all-gather.4.cloned.1.call-start
  98.7 0.1 convert_multiply_fusion
  98.8 3.4 %collective-permute-start = (f32[2,512]{1,0:T(2,128)S(1)}, f32[2,512]{1,0:T(2,128)S(1)}, u32[]{:S(2)}, u32[]{:S(2)}) collective-permute-start(f32[2,512]{1,0:T(2,128)S(1)} %slice.48), channel_id=1, source_target_pairs={{0,4},{4,8},{8,12},{12,16},{16,20},{20,24},{24,28},{1,5},{5,9},{9,... | collective-permute-start | bytes 12296 | tf_op jit(solution)/shard_map/ppermute | solution.py:13
  102.3 1.3 collective-permute-done
  103.5 1.2 fusion.20
  104.7 0.0 all-gather.4.cloned.1.call-update
  104.8 15.8 %all-gather.8.cloned.1.call-done = bf16[480,2048]{1,0:T(8,128)(2,1)} async-done(((bf16[480,512]{1,0:T(8,128)(2,1)}), bf16[480,2048]{1,0:T(8,128)(2,1)}) %all-gather.8.cloned.1.call-update) | async-done | bytes 1966096 | tf_op jit(solution)/shard_map/all_gather | solution.py:90
  120.6 5.0 %fusion.6 = bf16[480,1024]{1,0:T(8,128)(2,1)S(1)} fusion(bf16[480,2048]{1,0:T(8,128)(2,1)} %all-gather.8.cloned.1.call-done, bf16[1,2048,1024]{2,1,0:T(8,128)(2,1)} %param.25), kind=kOutput, calls=%fused_computation.10 | convolution fusion | flops 2013757440 | bytes 7143424 | tf_op jit(solution)/shard_map/dot_general | solution.py:89
  125.6 0.0 copy-start.4
  125.6 1.2 reshape.143
  126.8 5.5 %all-to-all-start.1 = ((bf16[8,60,1024]{2,1,0:T(8,128)(2,1)}), bf16[8,60,1024]{2,1,0:T(8,128)(2,1)S(1)}, u32[]{:S(2)}, u32[]{:S(2)}) async-start(bf16[8,60,1024]{2,1,0:T(8,128)(2,1)} %reshape.143), calls=%async_computation.1 | async-start | bytes 2097152 | tf_op jit(solution)/shard_map/all_to_all | solution.py:94
  132.3 0.1 copy.23
  132.5 12.9 %all-gather.4.cloned.1.call-done = bf16[512,2048]{1,0:T(8,128)(2,1)} async-done(((bf16[512,512]{1,0:T(8,128)(2,1)}), bf16[512,2048]{1,0:T(8,128)(2,1)}) %all-gather.4.cloned.1.call-update) | async-done | bytes 2097168 | tf_op jit(solution)/shard_map/all_gather | solution.py:58
  145.3 6.1 %convolution_convert_fusion = bf16[512,1024]{1,0:T(8,128)(2,1)} fusion(bf16[512,2048]{1,0:T(8,128)(2,1)} %all-gather.4.cloned.1.call-done, bf16[2048,1024]{1,0:T(8,128)(2,1)} %param.17), kind=kOutput, calls=%fused_computation.9 | convolution fusion | flops 2148007936 | bytes 7340032 | tf_op jit(solution)/shard_map/dot_general | solution.py:57
  151.5 7.0 %all-to-all-done.1 = bf16[8,60,1024]{2,1,0:T(8,128)(2,1)S(1)} async-done(((bf16[8,60,1024]{2,1,0:T(8,128)(2,1)}), bf16[8,60,1024]{2,1,0:T(8,128)(2,1)S(1)}, u32[]{:S(2)}, u32[]{:S(2)}) %all-to-all-start.1) | async-done | bytes 983072 | tf_op jit(solution)/shard_map/all_to_all | solution.py:94
  158.4 0.2 reshape.144
  158.6 2.1 %gather_fusion = bf16[320,1024]{1,0:T(8,128)(2,1)S(1)} fusion(bf16[480,1024]{1,0:T(8,128)(2,1)S(1)} %reshape.144, s32[1024]{0:T(1024)S(1)} %pad_clamp_fusion), kind=kCustom, calls=%fused_computation.1 | custom fusion | bytes 1312000 | tf_op jit(solution)/shard_map/gather | solution.py:102
  160.7 0.8 reshape.146
  161.5 2.4 %multiply_reduce_fusion = bf16[160,1024]{1,0:T(8,128)(2,1)} fusion(f32[160,2,1024]{2,1,0:T(2,128)S(1)} %reshape.146, f32[160,2]{1,0:T(8,128)S(1)} %copy.23), kind=kLoop, calls=%fused_computation.12 | loop fusion | flops 491520 | bytes 1639680 | tf_op jit(solution)/shard_map/reduce_sum | solution.py:107
  (24 shorter events, 0.2 us)
Async XLA Ops:
  7.2 82.8 %all-gather.6.cloned.1.call-start = ((), (), s32[]{:S(2)}) async-start(), calls=%async_computation.3 | async-start | bytes 4915200 | tf_op jit(solution)/shard_map/all_gather | solution.py:85
  57.7 62.9 %all-gather.8.cloned.1.call-start = ((), (), s32[]{:S(2)}) async-start(), calls=%async_computation.4 | async-start | bytes 2457600 | tf_op jit(solution)/shard_map/all_gather | solution.py:90
  89.9 3.4 %copy-start.6 = (bf16[1,4096,512]{2,1,0:T(8,128)(2,1)S(1)}, bf16[1,4096,512]{2,1,0:T(8,128)(2,1)}, u32[]{:S(2)}) copy-start(bf16[1,4096,512]{2,1,0:T(8,128)(2,1)} %param.23) | copy-start | bytes 12582916
  93.3 2.2 %copy-start.7 = (bf16[1,4096,512]{2,1,0:T(8,128)(2,1)S(1)}, bf16[1,4096,512]{2,1,0:T(8,128)(2,1)}, u32[]{:S(2)}) copy-start(bf16[1,4096,512]{2,1,0:T(8,128)(2,1)} %param.24) | copy-start | bytes 12582916
  95.5 3.2 %copy-start.1 = (bf16[512,512]{1,0:T(8,128)(2,1)S(1)}, bf16[512,512]{1,0:T(8,128)(2,1)}, u32[]{:S(2)}) copy-start(bf16[512,512]{1,0:T(8,128)(2,1)} %param.15) | copy-start | bytes 1572868
  95.5 3.2 %copy-start.2 = (bf16[512,512]{1,0:T(8,128)(2,1)S(1)}, bf16[512,512]{1,0:T(8,128)(2,1)}, u32[]{:S(2)}) copy-start(bf16[512,512]{1,0:T(8,128)(2,1)} %param.14) | copy-start | bytes 1572868
  95.5 6.7 %copy-start.3 = (f32[3,512]{1,0:T(4,128)S(1)}, f32[3,512]{1,0:T(4,128)}, u32[]{:S(2)}) copy-start(f32[3,512]{1,0:T(4,128)} %param.16) | copy-start | bytes 18436
  95.5 8.0 %copy-start = (bf16[512,512]{1,0:T(8,128)(2,1)S(1)}, bf16[512,512]{1,0:T(8,128)(2,1)}, u32[]{:S(2)}) copy-start(bf16[512,512]{1,0:T(8,128)(2,1)} %param.13) | copy-start | bytes 1572868
  98.6 46.7 %all-gather.4.cloned.1.call-start = ((), (), s32[]{:S(2)}) async-start(), calls=%async_computation.2 | async-start | bytes 2621440 | tf_op jit(solution)/shard_map/all_gather | solution.py:58
  98.8 4.7 %collective-permute-start = (f32[2,512]{1,0:T(2,128)S(1)}, f32[2,512]{1,0:T(2,128)S(1)}, u32[]{:S(2)}, u32[]{:S(2)}) collective-permute-start(f32[2,512]{1,0:T(2,128)S(1)} %slice.48), channel_id=1, source_target_pairs={{0,4},{4,8},{8,12},{12,16},{16,20},{20,24},{24,28},{1,5},{5,9},{9,... | collective-permute-start | bytes 12296 | tf_op jit(solution)/shard_map/ppermute | solution.py:13
  125.6 6.7 %copy-start.4 = (f32[160,2]{0,1:T(2,128)S(1)}, f32[160,2]{0,1:T(2,128)}, u32[]{:S(2)}) copy-start(f32[160,2]{0,1:T(2,128)} %param.22) | copy-start | bytes 3844
  125.6 6.7 %copy-start.5 = (f32[160]{0:T(256)S(1)}, f32[160]{0:T(256)}, u32[]{:S(2)}) copy-start(f32[160]{0:T(256)} %param.21) | copy-start | bytes 1924
  126.8 31.7 %all-to-all-start.1 = ((bf16[8,60,1024]{2,1,0:T(8,128)(2,1)}), bf16[8,60,1024]{2,1,0:T(8,128)(2,1)S(1)}, u32[]{:S(2)}, u32[]{:S(2)}) async-start(bf16[8,60,1024]{2,1,0:T(8,128)(2,1)} %reshape.143), calls=%async_computation.1 | async-start | bytes 2097152 | tf_op jit(solution)/shard_map/all_to_all | solution.py:94
Sparse Core Ops, SparseCore 0:
  57.8 32.0 all-gather.5
  98.7 21.8 all-gather.7
  122.7 22.5 all-gather.3
